TPU v7x, 512 devices: a 4x2x32 block of a 4x8x32 slice. The times are simulated.
512 devices in a mesh: grp: 2 (over y), sp: 32 (over z), tp: 8 (over x, core).
Axes of the slice: x: 4, y: 2, z: 32, core: 2. Of those that a mesh axis runs over, the one named last changes fastest.
The devices are a block of a 4x8x32 slice.
Arguments:
- queries: bfloat16 [32768, 1024], P(('grp', 'sp'), 'tp'), parts along dimension 0, may hold values from -6 to 6
- memory_keys: bfloat16 [32768, 1024], P(('grp', 'sp'), 'tp'), parts along dimension 0, may hold values from -6 to 6
- memory_values: bfloat16 [32768, 1024], P(('grp', 'sp'), 'tp'), parts along dimension 0, may hold values from -6 to 6
- output_preactivation: bfloat16 [32768, 1024], P(('grp', 'sp'), 'tp'), parts along dimension 0, may hold values from -12 to 12
- input_preactivation: float32 [8, 32768], P('tp', ('grp', 'sp')), parts along dimension 1, may hold values from -6 to 140
- forget_preactivation: float32 [8, 32768], P('tp', ('grp', 'sp')), parts along dimension 1, as said below
- extra_forget_terms: float32 [8, 32768], P('tp', ('grp', 'sp')), parts along dimension 1, may hold values from -1 to 0, as said below
- head_norm_gain: float32 [128], replicated, may hold values from 0.1 to 1.9
- output_projection_matrix: bfloat16 [1024, 2048], P('tp'), may hold values from -0.1875 to 0.1875
- residual: bfloat16 [32768, 2048], P(('grp', 'sp', 'tp')), parts along dimension 0, may hold values from -6 to 6
- feedforward_norm_gain: float32 [2048], replicated, may hold values from 0.1 to 1.9
- feedforward_up_matrix: bfloat16 [2048, 8192], P('sp', 'tp'), may hold values from -0.125 to 0.125
- feedforward_down_matrix: bfloat16 [8192, 2048], P('tp', 'sp'), may hold values from -0.0625 to 0.0625
Outputs:
- layer_out: bfloat16 [32768, 2048], P(('grp', 'sp', 'tp')), parts along dimension 0
There are 2 independent parts, one for each index of `grp`. A program takes and returns all parts, laid end to end along the dimension named above; an argument that names none is the same for every part. Nothing has to cross between parts.
Inputs may be any that keep to these rules, and one draw needn't show every extreme that they name: `forget_preactivation`: forget gate pre-activations. `extra_forget_terms`: extra log forget terms, zero at most positions.
All inputs are finite; a program needn't handle non-finite values.
Results may differ from a plain program's by a relative error of at most 0.018.
Values may be sent and summed in bfloat16 or wider, within the bound.
A program may use at most 64 MiB of HBM per device.

v0:
```python
import jax
import jax.numpy as jnp
from jax import lax
from jax.sharding import PartitionSpec as P

BLOCK = 128


neg_big = -1e30
norm_eps = 1e-06
highest = lax.Precision.HIGHEST


def turned_gather(arrays, axis, dims):
    turned = [jnp.moveaxis(a, dim, 0) for a, dim in zip(arrays, dims)]
    both = jnp.concatenate([t.reshape(len(t), -1) for t in turned], axis=1)
    filled, at, outs = (lax.all_gather(both, axis, axis=0, tiled=True), 0, [])
    for t, dim in zip(turned, dims):
        piece = filled[:, at : at + t[0].size].reshape(-1, *t.shape[1:])
        outs.append(jnp.moveaxis(piece, 0, dim))
        at += t[0].size
    return tuple(outs)


def all_in_one(x, axis):
    leaves = jax.tree.leaves(x)
    order = sorted(range(len(leaves)), key=lambda k: -leaves[k].size)
    width = (1, *leaves[order[0]].shape)[-1]
    lines = [
        jnp.pad(leaves[k].reshape(-1), (0, -leaves[k].size % width)).reshape(-1, width)
        for k in order
    ]
    both, at, found = (lax.all_gather(jnp.concatenate(lines), axis), 0, {})
    for k, line in zip(order, lines):
        piece = both[:, at : at + len(line)].reshape(len(both), -1)
        found[k] = piece[:, : leaves[k].size].reshape(-1, *leaves[k].shape)
        at += len(line)
    numbers = iter(range(len(leaves)))
    return jax.tree.map(lambda _: found[next(numbers)], x)


def prefix_2(part, axis, combine, identity):
    place = lax.axis_index(axis)
    gathered = all_in_one(part, axis)
    state = jax.tree.map(lambda a, e: jnp.zeros_like(a) + jnp.asarray(e, a.dtype), part, identity)

    def one(step, state):
        return combine(
            state, jax.tree.map(lambda a: lax.dynamic_index_in_dim(a, step, 0, False), gathered)
        )

    return lax.fori_loop(0, place, one, state)


def cut_along(x, dim, length):
    before, after = (x.shape[:dim], x.shape[dim + 1 :])
    return jnp.moveaxis(x.reshape(*before, length, -1, *after), dim, 0)


def sum_at_owner(x, axis, dim):
    length = lax.axis_size(axis)
    blocks = lax.all_to_all(cut_along(x, dim, length), axis, 0, 0, tiled=True)
    return jnp.sum(blocks.astype(jnp.float32), axis=0)


def laid_out(blocks, dim):
    blocks = jnp.moveaxis(blocks, 0, dim)
    lengths = blocks.shape
    return blocks.reshape(*lengths[:dim], lengths[dim] * lengths[dim + 1], *lengths[dim + 2 :])


def copy_for_each(x, axis):
    copies = jnp.broadcast_to(x, (lax.axis_size(axis), *x.shape))
    return lax.all_to_all(copies, axis, split_axis=0, concat_axis=0, tiled=True)


def gather_directly(x, axis, dim):
    return laid_out(copy_for_each(x, axis), dim)


def rms_norm(tensor, gain_vec):
    mean_sq = jnp.mean(tensor * tensor, axis=-1, keepdims=True)
    return tensor * lax.rsqrt(mean_sq + norm_eps) * gain_vec


def combine(earlier, later):
    total_e, max_e, memory_e = earlier
    total_l, max_l, memory_l = later
    carried = total_l + max_e
    new_max = jnp.maximum(carried, max_l)
    old_part = jnp.exp(carried - new_max)
    new_part = jnp.exp(max_l - new_max)
    return (
        total_e + total_l,
        new_max,
        old_part[..., None, None] * memory_e + new_part[..., None, None] * memory_l,
    )


def block_summary(key_blk, val_blk, gate_blk, decay_logarithm):
    block_total = decay_logarithm[..., -1]
    tail_log = block_total[..., None] - decay_logarithm + gate_blk
    tail_max = jnp.max(tail_log, axis=-1)
    weights = jnp.exp(tail_log - tail_max[..., None])
    memory = jnp.einsum("bhsv,bhsk->bhvk", weights[..., None] * val_blk, key_blk, precision=highest)
    return (block_total, tail_max, memory)


def shards(
    queries,
    memory_keys,
    memory_values,
    output_preactivation,
    input_preactivation,
    forget_preactivation,
    extra_forget_terms,
    head_norm_gain,
    output_projection_matrix,
    residual,
    feedforward_norm_gain,
    feedforward_up_matrix,
    feedforward_down_matrix,
):
    tok_count = queries.shape[0]
    head_count = input_preactivation.shape[0]
    head_dim = queries.shape[1] // head_count
    block_len = BLOCK
    block_count = tok_count // block_len
    whole_up, whole_down = turned_gather(
        (feedforward_up_matrix, feedforward_down_matrix), "sp", (0, 1)
    )

    def to_blocks(tensor):
        return (
            tensor.astype(jnp.float32)
            .reshape(block_count, block_len, head_count, head_dim)
            .transpose(0, 2, 1, 3)
        )

    def gate_block_list(tensor):
        return tensor.reshape(head_count, block_count, block_len).transpose(1, 0, 2)

    query_blk = to_blocks(queries)
    key_blk = to_blocks(memory_keys) * head_dim ** (-0.5)
    val_blk = to_blocks(memory_values)
    gate_blk = gate_block_list(input_preactivation)
    decay_logarithm = jnp.cumsum(
        gate_block_list(jax.nn.log_sigmoid(forget_preactivation) + extra_forget_terms), axis=-1
    )
    summaries = block_summary(key_blk, val_blk, gate_blk, decay_logarithm)
    zero_heads = jnp.zeros((head_count,), jnp.float32)
    zero_memory = jnp.zeros((head_count, head_dim, head_dim), jnp.float32)
    zero_state = (zero_heads, jnp.full((head_count,), neg_big, jnp.float32), zero_memory)
    prefixes = []
    running = zero_state
    for block_idx in range(block_count):
        prefixes.append(running)
        running = combine(running, tuple((member[block_idx] for member in summaries)))
    before = prefix_2(running, "sp", combine, zero_state)
    anchor = (zero_heads, zero_heads, zero_memory)
    incoming = combine(anchor, before)
    starts = [combine(incoming, prefix) for prefix in prefixes]
    start_max = jnp.stack([each_state[1] for each_state in starts])
    start_memory = jnp.stack([each_state[2] for each_state in starts])
    causal = lax.broadcasted_iota(jnp.int32, (block_len, block_len), 0) >= lax.broadcasted_iota(
        jnp.int32, (block_len, block_len), 1
    )
    log_weight = (
        decay_logarithm[..., :, None] - decay_logarithm[..., None, :] + gate_blk[..., None, :]
    )
    log_weight = jnp.where(causal, log_weight, neg_big)
    carry_log = decay_logarithm + start_max[..., None]
    row_max = jnp.maximum(jnp.max(log_weight, axis=-1), carry_log)
    scores = jnp.einsum("bhtd,bhsd->bhts", query_blk, key_blk, precision=highest) * jnp.exp(
        log_weight - row_max[..., None]
    )
    carry_scale = jnp.exp(carry_log - row_max)
    hidden = jnp.einsum("bhts,bhsv->bhtv", scores, val_blk, precision=highest)
    hidden = hidden + carry_scale[..., None] * jnp.einsum(
        "bhvk,bhtk->bhtv", start_memory, query_blk, precision=highest
    )
    hidden = hidden.transpose(0, 2, 1, 3).reshape(tok_count, head_count, head_dim)
    gated = rms_norm(hidden, head_norm_gain) * jax.nn.sigmoid(
        output_preactivation.astype(jnp.float32).reshape(tok_count, head_count, head_dim)
    )
    mixed = gated.reshape(tok_count, head_count * head_dim).astype(jnp.bfloat16)
    branch = sum_at_owner(
        jnp.dot(mixed, output_projection_matrix, preferred_element_type=jnp.float32).astype(
            jnp.bfloat16
        ),
        "tp",
        0,
    )
    mid_state = (residual.astype(jnp.float32) + branch).astype(jnp.bfloat16)
    normed = rms_norm(mid_state.astype(jnp.float32), feedforward_norm_gain).astype(jnp.bfloat16)
    normed_all = gather_directly(normed, "tp", 0)
    upward = jnp.dot(normed_all, whole_up, preferred_element_type=jnp.float32)
    active = jnp.square(jax.nn.relu(upward)).astype(jnp.bfloat16)
    mlp_sum = sum_at_owner(
        jnp.dot(active, whole_down, preferred_element_type=jnp.float32).astype(jnp.bfloat16),
        "tp",
        0,
    )
    return (mid_state.astype(jnp.float32) + mlp_sum).astype(jnp.bfloat16)


def solution(mesh):
    in_specs = (
        P(("grp", "sp"), "tp"),
        P(("grp", "sp"), "tp"),
        P(("grp", "sp"), "tp"),
        P(("grp", "sp"), "tp"),
        P("tp", ("grp", "sp")),
        P("tp", ("grp", "sp")),
        P("tp", ("grp", "sp")),
        P(),
        P("tp", None),
        P(("grp", "sp", "tp"), None),
        P(),
        P("sp", "tp"),
        P("tp", "sp"),
    )
    out_specs = P(("grp", "sp", "tp"), None)
    return jax.shard_map(shards, mesh=mesh, in_specs=in_specs, out_specs=out_specs, check_vma=False)
```

profile of v0, /device:TPU:33, one launch (start us, length us, event | category | flops | bytes accessed | tf_op | source)
XLA Modules:
  0.0 381.0 jit_solution(692592151489835851)
XLA Ops:
  6.5 0.0 copy-start
  6.6 0.0 copy-start.6
  6.6 0.0 all-gather.7.cloned.1.call-start
  6.6 0.8 fusion.40
  7.3 1.2 reduce_window_sum.11
  8.6 0.2 slice_reduce_fusion
  8.8 0.7 fusion.45
  9.4 0.9 fusion.39
  10.3 0.6 fusion.46
  19.9 0.9 convert_multiply_fusion.2
  22.1 0.8 subtract_exponential_fusion.1
  22.8 1.6 fusion.28
  24.5 0.6 maximum_bitcast_fusion.2
  25.1 0.1 all-gather.7.cloned.1.call-update
  25.2 0.1 all-gather.5.cloned.1.call-start
  25.2 1.7 pad_maximum_fusion
  26.9 0.1 all-gather.5.cloned.1.call-update
  27.0 0.0 copy-start.4
  27.0 0.1 copy.32
  27.2 0.0 copy-done.6
  27.2 0.2 select_reduce_fusion
  27.4 139.0 %all-gather.7.cloned.1.call-done = f32[32,130,128]{2,1,0:T(8,128)} async-done(((f32[1,130,128]{2,1,0:T(8,128)}), f32[32,130,128]{2,1,0:T(8,128)}) %all-gather.7.cloned.1.call-update) | async-done | bytes 2129936 | tf_op jit(solution)/shard_map/all_gather | solution.py:33
  166.4 0.0 copy-done.4
  166.4 1.7 fusion.44
  168.2 0.0 copy-start.2
  168.2 1.8 slice_bitcast_fusion
  169.9 0.0 copy-start.1
  170.0 0.0 copy-start.8
  170.0 0.0 copy-start.5
  171.1 0.1 maximum_bitcast_fusion.3
  171.2 0.1 subtract_exponential_fusion
  171.3 0.0 copy-done.2
  171.3 1.1 fusion.13
  172.4 0.0 copy-done.1
  172.5 0.4 fusion.47
  172.8 0.5 multiply_reduce_fusion
  173.4 0.0 copy-done.8
  173.4 0.0 copy-done.5
  173.4 0.1 fusion.27
  173.5 0.0 copy-done
  173.5 0.7 convolution_convert_fusion
  174.2 52.1 %all_to_all.15 = bf16[8,64,2048]{2,1,0:T(8,128)(2,1)S(1)} all-to-all(bf16[8,64,2048]{2,1,0:T(8,128)(2,1)S(1)} %bitcast.121), channel_id=1, replica_groups=mesh['grp'=2,'sp'=32,'tp'=8] {'tp'}, dimensions={0} | all-to-all | bytes 4194304 | tf_op jit(solution)/shard_map/all_to_all | solution.py:62
  226.3 0.0 copy-start.3
  226.4 0.0 copy-start.7
  226.4 0.4 convert_reduce_fusion.1
  226.7 0.6 copy-done.3
  227.3 0.2 fusion.15
  227.5 0.0 copy-done.7
  227.5 0.1 fusion.17
  227.6 0.2 broadcast_in_dim.21
  227.9 29.7 %all_to_all.16 = bf16[8,64,2048]{2,1,0:T(8,128)(2,1)S(1)} all-to-all(bf16[8,64,2048]{2,1,0:T(8,128)(2,1)S(1)} %broadcast_in_dim.21), channel_id=1, replica_groups=mesh['grp'=2,'sp'=32,'tp'=8] {'tp'}, dimensions={0} | all-to-all | bytes 4194304 | tf_op jit(solution)/shard_map/all_to_all | solution.py:74
  257.6 55.0 %all-gather.5.cloned.1.call-done = bf16[2048,2048]{1,0:T(8,128)(2,1)} async-done(((bf16[64,2048]{1,0:T(8,128)(2,1)}), bf16[2048,2048]{1,0:T(8,128)(2,1)}) %all-gather.5.cloned.1.call-update) | async-done | bytes 8388624 | tf_op jit(solution)/shard_map/all_gather | solution.py:17
  312.6 9.4 %fusion.4 = bf16[512,2048]{1,0:T(8,128)(2,1)} fusion(bf16[2048,2048]{1,0:T(8,128)(2,1)} %all-gather.5.cloned.1.call-done, bf16[512,2048]{1,0:T(8,128)(2,1)S(1)} %bitcast.124), kind=kOutput, calls=%fused_computation.9 | convolution fusion | flops 4297588736 | bytes 12582912 | tf_op jit(solution)/shard_map/dot_general | solution.py:200
  322.0 51.1 %all_to_all.17 = bf16[8,64,2048]{2,1,0:T(8,128)(2,1)S(1)} all-to-all(bf16[8,64,2048]{2,1,0:T(8,128)(2,1)} %bitcast.125), channel_id=1, replica_groups=mesh['grp'=2,'sp'=32,'tp'=8] {'tp'}, dimensions={0} | all-to-all | bytes 4194304 | tf_op jit(solution)/shard_map/all_to_all | solution.py:62
  373.0 0.4 convert_reduce_fusion
  373.4 0.8 fusion.18
  (8 shorter events, 0.1 us)
Async XLA Ops:
  6.5 167.0 %copy-start = (bf16[128,2048]{1,0:T(8,128)(2,1)S(1)}, bf16[128,2048]{1,0:T(8,128)(2,1)}, u32[]{:S(2)}) copy-start(bf16[128,2048]{1,0:T(8,128)(2,1)} %param.23) | copy-start | bytes 1572868
  6.6 20.6 %copy-start.6 = (f32[1,512]{1,0:T(1,128)S(1)}, f32[1,512]{1,0:T(1,128)}, u32[]{:S(2)}) copy-start(f32[1,512]{1,0:T(1,128)} %param.19) | copy-start | bytes 6148
  6.6 159.9 %all-gather.7.cloned.1.call-start = ((), (), s32[]{:S(2)}) async-start(), calls=%async_computation.4 | async-start | bytes 2297856 | tf_op jit(solution)/shard_map/all_gather | solution.py:33
  25.2 287.4 %all-gather.5.cloned.1.call-start = ((), (), s32[]{:S(2)}) async-start(), calls=%async_computation.3 | async-start | bytes 8650752 | tf_op jit(solution)/shard_map/all_gather | solution.py:17
  27.0 139.4 %copy-start.4 = (pred[128,128]{0,1:T(8,128)(4,1)}, pred[128,128]{0,1:T(8,128)(4,1)S(1)}, u32[]{:S(2)}) copy-start(pred[128,128]{0,1:T(8,128)(4,1)S(1)} %iota_compare_fusion) | copy-start | bytes 49156
  168.2 3.2 copy-start.2
  169.9 2.5 copy-start.1
  170.0 3.4 copy-start.8
  170.0 3.4 copy-start.5
  226.3 1.0 copy-start.3
  226.4 1.1 copy-start.7
Sparse Core Ops, SparseCore 0:
  25.3 141.1 all-gather.6
  168.5 144.0 all-gather.4
where the time goes:
time: 385 us; the launch traced here: 381 us
  waiting for transfers between devices  194 us (50%)
  blocking collectives  133 us (35%)
  between operations  25 us (6%)
  matrix products  13.7 us (4%)
  other arithmetic  9.31 us (2%)
  local copies, waits for them, and re-layouts  5.93 us (2%)
    all_gather x1, waiting for transfers between devices, all_in_one(): both, at, found = (lax.all_gather(jnp.concatenate(lines), axis), 0, {})  139 us
    all_to_all x2, blocking collectives, sum_at_owner(): blocks = lax.all_to_all(cut_along(x, dim, length), axis, 0, 0, tiled=True)  103 us
    all_gather x1, waiting for transfers between devices, turned_gather(): filled, at, outs = (lax.all_gather(both, axis, axis=0, tiled=True), 0, [])  55 us
    all_to_all x1, blocking collectives, copy_for_each(): return lax.all_to_all(copies, axis, split_axis=0, concat_axis=0, tiled=True)  29.7 us
    dot_general x1, matrix products, shards(): jnp.dot(active, whole_down, preferred_element_type=jnp.float32)  9.37 us
  transfers between devices with their start and end apart: 2, of which 2 were waited for; matrix products, arithmetic and copies ran while one was open for 2% of the time, Pallas kernels for 0%

commit v1 on v0

v1 whole, which is shorter than its diff:
```python
import functools

import jax
import jax.numpy as jnp
from jax import lax
from jax.experimental import pallas as pl
from jax.experimental.pallas import tpu as pltpu
from jax.sharding import PartitionSpec as P

BLOCK = 128
CORES = 2
SUB = 4
UNIT = 16
NORM_EPS = 1e-06
NEG_BIG = -1e30
MESH = pl.DeviceIdType.MESH
F32 = jnp.float32
BF16 = jnp.bfloat16


def two_part_dot(a, b, dims=(((1,), (0,)), ((), ()))):
    high = a.astype(BF16)
    low = (a - high.astype(F32)).astype(BF16)
    dot = functools.partial(lax.dot_general, dimension_numbers=dims, preferred_element_type=F32)
    return dot(high, b) + dot(low, b)


def dot_two_part(a, b):
    high = b.astype(BF16)
    low = (b - high.astype(F32)).astype(BF16)
    return jnp.dot(a, high, preferred_element_type=F32) + jnp.dot(a, low, preferred_element_type=F32)


def rem(a, b):
    return lax.rem(a, jnp.int32(b))


def kernel(
    sizes,
    q_ref, k_ref, v_ref, og_ref, ig_ref, fg_ref, ex_ref, hng_ref, wo_in, res_in, fng_ref, up_in, dn_in,
    out_ref,
    UP, DN, WO, RES, MIX, MID, NRM, SSQ, ACT, PART, SIB, SUM, RSR, LM, ST, AS, AR, GX, BS, BR, CS, CR,
    SR, RR, SL, RL, SY, RYU, RYD, SX, RX, SD, RD, SA, RA, SB, RB, SC, RC, SP, RP, SQ, RQ,
):
    nz, nt, share = sizes
    nx = nt // CORES
    ng = nz // SUB
    n_right, n_left = nz // 2, nz - 1 - nz // 2
    tok, dh = q_ref.shape
    nb = tok // BLOCK
    width = res_in.shape[1]
    own_rows = res_in.shape[0]
    wrows, hid = up_in.shape
    gcols = SUB * wrows

    me, t, grp = lax.axis_index("sp"), lax.axis_index("tp"), lax.axis_index("grp")
    x, c = lax.div(t, jnp.int32(CORES)), rem(t, CORES)
    sib = x * CORES + 1 - c
    parity = rem(grp, 2)
    pair = grp + 1 - 2 * parity
    right, left = rem(me + 1, nz), rem(me + nz - 1, nz)
    gz, j = lax.div(me, jnp.int32(SUB)), rem(me, SUB)

    def remote(src, dst, send, recv, **device):
        return pltpu.make_async_remote_copy(
            src_ref=src, dst_ref=dst, send_sem=send, recv_sem=recv, device_id=device, device_id_type=MESH
        )

    def drain(ref, sem):
        pltpu.make_async_copy(ref, ref, sem).wait()

    barrier = pltpu.get_barrier_semaphore()
    others = [dict(sp=right), dict(sp=left), dict(sp=rem(me + SUB, nz)), dict(sp=rem(me + nz - SUB, nz))]
    others += [dict(sp=gz * SUB + rem(j + d, SUB)) for d in range(1, SUB)]
    others += [dict(tp=rem(x + d, nx) * CORES + c) for d in range(1, nx)]
    others += [dict(tp=sib)]
    if share:
        others += [dict(grp=pair)]
    for device in others:
        pl.semaphore_signal(barrier, inc=1, device_id=device, device_id_type=MESH)
    pl.semaphore_wait(barrier, len(others))

    if share:
        offsets = [2 * UNIT, 3 * UNIT, parity * UNIT]
    else:
        offsets = [0, UNIT, 2 * UNIT, 3 * UNIT]
    n_pieces = len(offsets)
    weights, own_w = (UP, DN), (up_in, dn_in)

    def piece(ph, origin, i):
        return weights[ph].at[pl.ds(pl.multiple_of(origin * wrows + offsets[i], UNIT), UNIT), :]

    def hop0(ph):
        for i in range(n_pieces):
            src = own_w[ph].at[pl.ds(pl.multiple_of(offsets[i] + 0 * me, UNIT), UNIT), :]
            remote(src, piece(ph, me, i), SR.at[ph, i], RR.at[ph, i, 1], sp=right).start()
            remote(src, piece(ph, me, i), SL.at[ph, i], RL.at[ph, i, 1], sp=left).start()

    def to_pair(ph, origin):
        if ph == 0:
            sem = RYU.at[0]
        else:
            sem = RYD.at[rem(lax.div(origin, jnp.int32(SUB)) - gz + ng, ng)]
        part = piece(ph, origin, n_pieces - 1)
        remote(part, part, SY.at[ph], sem, grp=pair).start()

    def tick(ph, h):
        from_left, from_right = rem(me - h + nz, nz), rem(me + h, nz)
        for i in reversed(range(n_pieces)):
            a, b = piece(ph, from_left, i), piece(ph, from_right, i)
            remote(a, a, SR.at[ph, i], RR.at[ph, i, h], sp=right).wait_recv()

            @pl.when(h < n_right)
            def _():
                remote(a, a, SR.at[ph, i], RR.at[ph, i, h + 1], sp=right).start()

            if share and i == n_pieces - 1:
                to_pair(ph, from_left)

            @pl.when(h <= n_left)
            def _():
                remote(b, b, SL.at[ph, i], RL.at[ph, i, h], sp=left).wait_recv()

                @pl.when(h < n_left)
                def _():
                    remote(b, b, SL.at[ph, i], RL.at[ph, i, h + 1], sp=left).start()

                if share and i == n_pieces - 1:
                    to_pair(ph, from_right)

    def ticks(ph, first, last):
        def body(h, _):
            tick(ph, h)
            return 0

        lax.fori_loop(first, last + 1, body, 0)

    hop0(0)

    waits = []

    def wo_rows(s):
        return WO.at[pl.ds(pl.multiple_of(s * dh, dh), dh), :]

    def res_rows(s):
        return RES.at[pl.ds(pl.multiple_of(s * own_rows, own_rows), own_rows), :]

    def mix_cols(s):
        return MIX.at[:, pl.ds(pl.multiple_of(s * dh, dh), dh)]

    def spread(which, own, region):
        for d in [2, 1, 3, *range(4, nx)]:
            if d < nx:
                copy = remote(own, region(t), SX.at[which, d], RX.at[which, d], tp=rem(x + d, nx) * CORES + c)
                copy.start()
                waits.append(copy)
        copy = remote(own, region(t), SD.at[which, 0], RD.at[which, 0], tp=sib)
        copy.start()
        waits.append(copy)

    def pass_on(which, region):
        for d in range(1, nx):
            part = region(rem(x - d + nx, nx) * CORES + c)
            remote(part, part, SX.at[which, d], RX.at[which, d], tp=sib).wait_recv()
            copy = remote(part, part, SD.at[which, d], RD.at[which, d], tp=sib)
            copy.start()
            waits.append(copy)

    def passed(which, region):
        for d in range(nx):
            part = region(rem(x - d + nx, nx) * CORES + 1 - c)
            remote(part, part, SD.at[which, d], RD.at[which, d], tp=sib).wait_recv()

    spread(0, res_in, res_rows)
    spread(1, wo_in, wo_rows)

    lane = lax.broadcasted_iota(jnp.int32, (1, BLOCK), 1)
    scale = dh ** (-0.5)
    total = top = memory = None
    for b in range(nb):
        cols = slice(b * BLOCK, (b + 1) * BLOCK)
        f = fg_ref[:, cols]
        cum = jnp.minimum(f, 0.0) - jnp.log1p(jnp.exp(-jnp.abs(f))) + ex_ref[:, cols]
        step = 1
        while step < BLOCK:
            cum = cum + jnp.where(lane >= step, pltpu.roll(cum, step, 1), 0.0)
            step *= 2
        ST[b : b + 1, :] = cum
        whole = jnp.sum(jnp.where(lane == BLOCK - 1, cum, 0.0), axis=1, keepdims=True)
        tail = whole - cum + ig_ref[:, cols]
        tail_top = jnp.max(tail, axis=1, keepdims=True)
        weight = jnp.exp(tail - tail_top)
        keys_t = k_ref[cols, :].astype(F32).T
        part = two_part_dot(keys_t * weight, v_ref[cols, :]) * scale
        if b == 0:
            total, top, memory = whole, tail_top, part
        else:
            LM[b - 1] = memory
            ST[8 + b : 9 + b, :] = jnp.broadcast_to(total, (1, BLOCK))
            ST[16 + b : 17 + b, :] = jnp.broadcast_to(top, (1, BLOCK))
            new_top = jnp.maximum(whole + top, tail_top)
            memory = jnp.exp(whole + top - new_top) * memory + jnp.exp(tail_top - new_top) * part
            total, top = total + whole, new_top
    srows = dh // SUB
    for i in range(SUB):
        AS[i, 0:srows, :] = memory[i * srows : (i + 1) * srows, :]
        AS[i, srows : srows + 1, :] = jnp.broadcast_to(total, (1, dh))
        AS[i, srows + 1 : srows + 2, :] = jnp.broadcast_to(top, (1, dh))
    for d in range(1, SUB):
        i = rem(j + d, SUB)
        copy = remote(AS.at[i], AR.at[j], SA.at[d], RA.at[d], sp=gz * SUB + i)
        copy.start()
        waits.append(copy)
    AR[j] = AS[j]
    UP[pl.ds(pl.multiple_of(me * wrows, wrows), wrows), :] = up_in[...]
    DN[pl.ds(pl.multiple_of(me * wrows, wrows), wrows), :] = dn_in[...]
    WO[pl.ds(pl.multiple_of(t * dh, dh), dh), :] = wo_in[...]
    RES[pl.ds(pl.multiple_of(t * own_rows, own_rows), own_rows), :] = res_in[...]

    first = n_right - 2 * (ng - 1)
    ticks(0, 1, first)
    for d in range(1, SUB):
        slot = AR.at[rem(j - d + SUB, SUB)]
        remote(slot, slot, SA.at[d], RA.at[d], sp=right).wait_recv()

    def member(i):
        return AR[i, 0:srows, :], AR[i, srows : srows + 1, :], AR[i, srows + 1 : srows + 2, :]

    def fold(state, top, member_state):
        part, part_total, part_top = member_state
        new_top = jnp.maximum(part_total + top, part_top)
        return jnp.exp(part_total + top - new_top) * state + jnp.exp(part_top - new_top) * part, new_top

    g_state, g_total, g_top = member(0)
    for i in range(1, SUB):
        m_state = member(i)
        g_state, g_top = fold(g_state, g_top, m_state)
        g_total = g_total + m_state[1]
    GX[0:srows, :] = g_state
    GX[srows : srows + 1, :] = g_total
    GX[srows + 1 : srows + 2, :] = g_top

    def chain(r):
        @pl.when(gz == r)
        def _():
            @pl.when(gz > 0)
            def _():
                remote(BR, BR, SB.at[0], RB.at[0], sp=right).wait_recv()

            @pl.when(gz == 0)
            def _():
                BR[...] = jnp.zeros_like(BR)

            state, top = BR[0:srows, :], BR[srows + 1 : srows + 2, :]
            after, after_top = fold(
                state, top, (GX[0:srows, :], GX[srows : srows + 1, :], GX[srows + 1 : srows + 2, :])
            )
            BS[0:srows, :] = after
            BS[srows + 1 : srows + 2, :] = after_top

            @pl.when(gz < ng - 1)
            def _():
                remote(BS, BR, SB.at[0], RB.at[0], sp=rem(me + SUB, nz)).start()

            for i in range(SUB):
                CS[i, 0:srows, :] = state
                CS[i, srows + 1 : srows + 2, :] = top
                if i < SUB - 1:
                    state, top = fold(state, top, member(i))
            for d in range(1, SUB):
                i = rem(j + d, SUB)
                remote(CS.at[i], CR.at[j], SC.at[d], RC.at[d], sp=gz * SUB + i).start()
            CR[j] = CS[j]

    def chain_step(r, _):
        chain(r)
        tick(0, first + 1 + 2 * r)
        tick(0, first + 2 + 2 * r)
        return 0

    lax.fori_loop(0, ng - 2, chain_step, 0)
    hop0(1)
    chain_step(ng - 2, 0)
    chain(ng - 1)
    pass_on(0, res_rows)
    pass_on(1, wo_rows)
    tick(1, 1)

    for d in range(1, SUB):
        slot = CR.at[rem(j - d + SUB, SUB)]
        remote(slot, slot, SC.at[d], RC.at[d], sp=right).wait_recv()
    before = jnp.concatenate([CR[i, 0:srows, :] for i in range(SUB)], axis=0)
    before_top = CR[0, srows + 1 : srows + 2, :]
    causal = lax.broadcasted_iota(jnp.int32, (BLOCK, BLOCK), 0) >= lax.broadcasted_iota(
        jnp.int32, (BLOCK, BLOCK), 1
    )
    mine = pl.ds(pl.multiple_of(t * dh, dh), dh)
    for b in range(nb):
        cols = slice(b * BLOCK, (b + 1) * BLOCK)
        cum = ST[b : b + 1, :]
        if b == 0:
            start, start_top = before, before_top
        else:
            total, top = ST[8 + b : 9 + b, :], ST[16 + b : 17 + b, :]
            start_top = jnp.maximum(total + before_top, top)
            start = jnp.exp(total + before_top - start_top) * before + jnp.exp(top - start_top) * LM[b - 1]
        cum_t = jnp.broadcast_to(cum, (BLOCK, BLOCK)).T
        log_weight = jnp.where(causal, cum_t - cum + ig_ref[:, cols], NEG_BIG)
        carry_log = cum_t + start_top
        row_max = jnp.maximum(jnp.max(log_weight, axis=1, keepdims=True), carry_log)
        q, k, v = q_ref[cols, :], k_ref[cols, :], v_ref[cols, :]
        qk = lax.dot_general(q, k, (((1,), (1,)), ((), ())), preferred_element_type=F32) * scale
        hidden = two_part_dot(qk * jnp.exp(log_weight - row_max), v)
        hidden = hidden + jnp.exp(carry_log - row_max) * dot_two_part(q, start)
        mean_sq = jnp.mean(hidden * hidden, axis=1, keepdims=True)
        gate = jax.nn.sigmoid(og_ref[cols, :].astype(F32))
        mixed = hidden * lax.rsqrt(mean_sq + NORM_EPS) * hng_ref[...] * gate
        MIX[cols, mine] = mixed.astype(BF16)
    spread(2, mix_cols(t), mix_cols)
    ticks(1, 2, 4)
    pass_on(2, mix_cols)
    for which, region in ((0, res_rows), (1, wo_rows)):
        passed(which, region)
    tick(1, 5)
    passed(2, mix_cols)

    SSQ[...] = jnp.zeros_like(SSQ)

    def project(n, _):
        at = pl.ds(pl.multiple_of(n * 256, 256), 256)
        branch = jnp.dot(MIX[...], WO[:, at], preferred_element_type=F32)
        mid = (RES[:, at].astype(F32) + branch).astype(BF16)
        MID[:, at] = mid
        wide = mid.astype(F32)
        SSQ[...] += wide[:, :128] * wide[:, :128] + wide[:, 128:] * wide[:, 128:]
        return 0

    n_cols = width // 256
    for n in range(0, n_cols, 4):
        lax.fori_loop(n, n + 4, project, 0)
        tick(1, 6 + n // 4)

    def normalize(n, _):
        at = pl.ds(pl.multiple_of(n * 64, 64), 64)
        mean_sq = jnp.sum(SSQ[at, :], axis=1, keepdims=True) / width
        NRM[at, :] = (MID[at, :].astype(F32) * lax.rsqrt(mean_sq + NORM_EPS) * fng_ref[...]).astype(BF16)
        return 0

    lax.fori_loop(0, tok // 64, normalize, 0)
    tick(1, 8)

    if share:
        drain(UP.at[pl.ds(0, (nz - 1) * UNIT), :], RYU.at[0])

    def upward(n, _):
        at = pl.ds(pl.multiple_of(n * 256, 256), 256)
        value = jnp.maximum(jnp.dot(NRM[...], UP[:, at], preferred_element_type=F32), 0.0)
        ACT[:, at] = (value * value).astype(BF16)
        return 0

    for n in range(0, hid // 256, 2):
        lax.fori_loop(n, n + 2, upward, 0)
        tick(1, 9 + n // 2)

    def group_of(k):
        return rem(gz + k, ng)

    def down(k):
        if share:
            drain(DN.at[pl.ds(0, (SUB if k else SUB - 1) * UNIT), :], RYD.at[k])
        rows = pl.ds(pl.multiple_of(group_of(k) * gcols, gcols), gcols)
        value = lax.dot_general(
            ACT[...], DN[rows, :], (((1,), (1,)), ((), ())), preferred_element_type=F32
        )
        PART[k] = value.astype(BF16).reshape(nx, CORES, own_rows, gcols)
        copy = remote(PART.at[k, :, 1 - c], SIB.at[k], SP.at[k], RP.at[k], tp=sib)
        copy.start()
        waits.append(copy)

    def add_up(k):
        remote(SIB.at[k], SIB.at[k], SP.at[k], RP.at[k], tp=sib).wait_recv()
        for i in range(nx):
            SUM[k, i] = (PART[k, i, c].astype(F32) + SIB[k, i].astype(F32)).astype(BF16)
        for d in [2, 1, 3, *range(4, nx)]:
            if d < nx:
                i = rem(x + d, nx)
                copy = remote(SUM.at[k, i], RSR.at[k, x], SQ.at[k, d], RQ.at[k, d], tp=i * CORES + c)
                copy.start()
                waits.append(copy)

    def finish(k):
        at = pl.ds(pl.multiple_of(group_of(k) * gcols, gcols), gcols)
        value = MID[pl.ds(pl.multiple_of(t * own_rows, own_rows), own_rows), at].astype(F32)
        value = value + SUM[k, x].astype(F32)
        for d in range(1, nx):
            slot = RSR.at[k, rem(x - d + nx, nx)]
            remote(slot, slot, SQ.at[k, d], RQ.at[k, d], tp=sib).wait_recv()
            value = value + RSR[k, rem(x - d + nx, nx)].astype(F32)
        out_ref[:, at] = value.astype(BF16)

    done, order = 8 + hid // 512, []
    plan = [(0, 3)]
    for s in range(1, ng // 2):
        plan += [(ng - s, SUB * s + 3), (s, SUB * s + 3)]
    plan += [(ng // 2, n_right)]
    late = 0
    for n, (k, need) in enumerate(plan):
        while done < need:
            done += 1
            tick(1, done)
        down(k)
        if done < n_right and n < len(plan) - 1 and done < 14:
            done += 1
            tick(1, done)
        order.append(k)
        if n > 0:
            add_up(order[n - 1])
        if n > 3:
            finish(order[late])
            late += 1
    add_up(order[-1])
    for k in order[late:]:
        finish(k)

    for ph in range(2):
        for i in range(n_pieces):
            drain(weights[ph].at[pl.ds(0, n_right * UNIT), :], SR.at[ph, i])
            drain(weights[ph].at[pl.ds(0, n_left * UNIT), :], SL.at[ph, i])
        if share:
            drain(weights[ph].at[pl.ds(0, (nz - 1) * UNIT), :], SY.at[ph])
    for copy in waits:
        copy.wait_send()
    for d in range(1, SUB):
        drain(CS.at[0], SC.at[d])

    @pl.when(gz < ng - 1)
    def _():
        drain(BS, SB.at[0])


def shards(
    sizes,
    queries,
    memory_keys,
    memory_values,
    output_preactivation,
    input_preactivation,
    forget_preactivation,
    extra_forget_terms,
    head_norm_gain,
    output_projection_matrix,
    residual,
    feedforward_norm_gain,
    feedforward_up_matrix,
    feedforward_down_matrix,
):
    nz, nt, share = sizes
    nx, ng = nt // CORES, nz // SUB
    tok, dh = queries.shape
    own_rows, width = residual.shape
    wrows, hid = feedforward_up_matrix.shape
    n_right = nz // 2
    n_pieces = 3 if share else 4
    gcols = SUB * wrows
    msg = (dh // SUB + 8, dh)
    dma = pltpu.SemaphoreType.DMA
    vmem = pltpu.VMEM
    scratch = [
        vmem((nz * wrows, hid), BF16),
        vmem((nz * wrows, hid), BF16),
        vmem((nt * dh, width), BF16),
        vmem((tok, width), BF16),
        vmem((tok, nt * dh), BF16),
        vmem((tok, width), BF16),
        vmem((tok, width), BF16),
        vmem((tok, 128), F32),
        vmem((tok, hid), BF16),
        vmem((ng, nx, CORES, own_rows, gcols), BF16),
        vmem((ng, nx, own_rows, gcols), BF16),
        vmem((ng, nx, own_rows, gcols), BF16),
        vmem((ng, nx, own_rows, gcols), BF16),
        vmem((tok // BLOCK - 1, dh, dh), F32),
        vmem((24, BLOCK), F32),
        vmem((SUB, *msg), F32),
        vmem((SUB, *msg), F32),
        vmem(msg, F32),
        vmem(msg, F32),
        vmem(msg, F32),
        vmem((SUB, *msg), F32),
        vmem((SUB, *msg), F32),
        dma((2, n_pieces)),
        dma((2, n_pieces, n_right + 1)),
        dma((2, n_pieces)),
        dma((2, n_pieces, n_right + 1)),
        dma((2,)),
        dma((1,)),
        dma((ng,)),
        dma((3, nx)),
        dma((3, nx)),
        dma((3, nx)),
        dma((3, nx)),
        dma((SUB,)),
        dma((SUB,)),
        dma((1,)),
        dma((1,)),
        dma((SUB,)),
        dma((SUB,)),
        dma((ng,)),
        dma((ng,)),
        dma((ng, nx)),
        dma((ng, nx)),
    ]
    return pl.pallas_call(
        functools.partial(kernel, sizes),
        out_shape=jax.ShapeDtypeStruct((own_rows, width), BF16),
        in_specs=[pl.BlockSpec(memory_space=pltpu.VMEM)] * 13,
        out_specs=pl.BlockSpec(memory_space=pltpu.VMEM),
        scratch_shapes=scratch,
        compiler_params=pltpu.CompilerParams(
            collective_id=0, has_side_effects=True, vmem_limit_bytes=56 * 1024 * 1024
        ),
        name="layer",
    )(
        queries,
        memory_keys,
        memory_values,
        output_preactivation,
        input_preactivation,
        forget_preactivation,
        extra_forget_terms,
        head_norm_gain.reshape(1, -1),
        output_projection_matrix,
        residual,
        feedforward_norm_gain.reshape(1, -1),
        feedforward_up_matrix,
        feedforward_down_matrix.T,
    )


def solution(mesh):
    in_specs = (
        P(("grp", "sp"), "tp"),
        P(("grp", "sp"), "tp"),
        P(("grp", "sp"), "tp"),
        P(("grp", "sp"), "tp"),
        P("tp", ("grp", "sp")),
        P("tp", ("grp", "sp")),
        P("tp", ("grp", "sp")),
        P(),
        P("tp", None),
        P(("grp", "sp", "tp"), None),
        P(),
        P("sp", "tp"),
        P("tp", "sp"),
    )
    out_specs = P(("grp", "sp", "tp"), None)
    sizes = (mesh.shape["sp"], mesh.shape["tp"], mesh.shape["grp"] % 2 == 0)
    return jax.shard_map(
        functools.partial(shards, sizes), mesh=mesh, in_specs=in_specs, out_specs=out_specs, check_vma=False
    )
```

time: 385 us -> 174 us (0.45)
  waiting for transfers between devices: 194 us -> 0 us
  Pallas kernels: 0 us -> 172 us
  blocking collectives: 133 us -> 0 us
  between operations: 25 us -> 0.01 us
  matrix products: 13.7 us -> 0 us
  other arithmetic: 9.31 us -> 0 us
  local copies, waits for them, and re-layouts: 5.93 us -> 1.67 us
    all_gather x2 -> x0, waiting for transfers between devices: 194 us -> none  [the longest x1 139 us: all_in_one(): both, at, found = (lax.all_gather(jnp.concatenate(lines), axis), 0, {})]
    pallas_call x0 -> x1, Pallas kernels: none -> 172 us  [shards(): pl.pallas_call(functools.partial(kernel, sizes), out_shape=jax.ShapeDtype...]
    all_to_all x3 -> x0, blocking collectives: 133 us -> none  [the longest x2 103 us: sum_at_owner(): blocks = lax.all_to_all(cut_along(x, dim, length), axis, 0, 0, tiled=True)]
    dot_general x6 -> x0, matrix products: 13.7 us -> none  [the longest x1 9.37 us: shards(): jnp.dot(active, whole_down, preferred_element_type=jnp.float32)]
  transfers between devices with their start and end apart: 2 -> 0, of which waited for: 2 -> 0; matrix products, arithmetic and copies ran while one was open for 2% -> 0% of each run, Pallas kernels for 0% -> 0%
where the time goes in v1:
time: 174 us
  Pallas kernels  172 us (99%)
    pallas_call x1, Pallas kernels, shards(): pl.pallas_call(functools.partial(kernel, sizes), out_shape=jax.ShapeDtype...  172 us

profile of v1, /device:TPU:33, one launch (start us, length us, event | category | flops | bytes accessed | tf_op | source)
XLA Modules:
  0.0 173.7 jit_solution(280371460621154627)
XLA Ops:
  0.0 172.0 %layer.1 = bf16[64,2048]{1,0:T(8,128)(2,1)} custom-call(bf16[512,128]{1,0:T(8,128)(2,1)} %q_ref.1, bf16[512,128]{1,0:T(8,128)(2,1)} %k_ref.1, bf16[512,128]{1,0:T(8,128)(2,1)} %v_ref.1, bf16[512,128]{1,0:T(8,128)(2,1)} %og_ref.1, f32[1,512]{1,0:T(1,128)} %ig_ref.1, f32[1,512]{1,0:T(1,128)} %fg_ref.1, f32[1,512]{1,0:T(1,128)} %ex_ref.1, f32[1,128]{1,0:T(1,128)} %bitcast.5, ...), custom_call_target="tpu_custom_call" | custom-call | tf_op jit(solution)/shard_map/layer/pallas_call | solution.py:513
  172.1 1.7 copy.15

commit v2 on v1

--- a/solution.py
+++ b/solution.py
@@ -8,6 +8,7 @@
 from jax.sharding import PartitionSpec as P
 
 BLOCK = 128
+CHAIN_LATE = 7
 CORES = 2
 SUB = 4
 UNIT = 16
@@ -39,8 +40,8 @@
     sizes,
     q_ref, k_ref, v_ref, og_ref, ig_ref, fg_ref, ex_ref, hng_ref, wo_in, res_in, fng_ref, up_in, dn_in,
     out_ref,
-    UP, DN, WO, RES, MIX, MID, NRM, SSQ, ACT, PART, SIB, SUM, RSR, LM, ST, AS, AR, GX, BS, BR, CS, CR,
-    SR, RR, SL, RL, SY, RYU, RYD, SX, RX, SD, RD, SA, RA, SB, RB, SC, RC, SP, RP, SQ, RQ,
+    UP, DN, WO, RES, MIX, MID, NRM, SSQ, UACC, ACT, PART, SIB, SUM, RSR, LM, ST, AS, AR, GX, BS, BR, CS, CR,
+    SR, RR, SL, RL, SY, RY, SX, RX, SD, RD, SA, RA, SB, RB, SC, RC, SP, RP, SQ, RQ,
 ):
     nz, nt, share = sizes
     nx = nt // CORES
@@ -80,33 +81,56 @@
         pl.semaphore_signal(barrier, inc=1, device_id=device, device_id_type=MESH)
     pl.semaphore_wait(barrier, len(others))
 
+    hid_half = hid // 2
     if share:
-        offsets = [2 * UNIT, 3 * UNIT, parity * UNIT]
+        mine_row, mine_col = parity * UNIT, parity * hid_half
+        cuts = (
+            [(3 * UNIT, 0, hid, False), (2 * UNIT, mine_col, hid_half, True), (mine_row, 0, hid, True)],
+            [(2 * UNIT, 0, hid, False), (3 * UNIT, 0, hid, False), (mine_row, 0, hid, True)],
+        )
+        order = [(0, 2), (1, 2), (0, 1), (1, 1), (0, 0), (1, 0)]
     else:
-        offsets = [0, UNIT, 2 * UNIT, 3 * UNIT]
-    n_pieces = len(offsets)
+        cuts = ([(i * UNIT, 0, hid, False) for i in range(4)],) * 2
+        order = [(ph, i) for i in range(4) for ph in range(2)]
     weights, own_w = (UP, DN), (up_in, dn_in)
 
+    def region(ref, start, ph, i):
+        row, col, n_col, _ = cuts[ph][i]
+        row = pl.multiple_of(start + row, UNIT)
+        if n_col == hid:
+            return ref.at[pl.ds(row, UNIT), :]
+        return ref.at[pl.ds(row, UNIT), pl.ds(pl.multiple_of(col, 128), n_col)]
+
     def piece(ph, origin, i):
-        return weights[ph].at[pl.ds(pl.multiple_of(origin * wrows + offsets[i], UNIT), UNIT), :]
-
-    def hop0(ph):
-        for i in range(n_pieces):
-            src = own_w[ph].at[pl.ds(pl.multiple_of(offsets[i] + 0 * me, UNIT), UNIT), :]
-            remote(src, piece(ph, me, i), SR.at[ph, i], RR.at[ph, i, 1], sp=right).start()
-            remote(src, piece(ph, me, i), SL.at[ph, i], RL.at[ph, i, 1], sp=left).start()
-
-    def to_pair(ph, origin):
-        if ph == 0:
-            sem = RYU.at[0]
-        else:
-            sem = RYD.at[rem(lax.div(origin, jnp.int32(SUB)) - gz + ng, ng)]
-        part = piece(ph, origin, n_pieces - 1)
-        remote(part, part, SY.at[ph], sem, grp=pair).start()
-
-    def tick(ph, h):
+        return region(weights[ph], origin * wrows, ph, i)
+
+    def hop0(ph, i):
+        src = region(own_w[ph], 0 * me, ph, i)
+        remote(src, piece(ph, me, i), SR.at[ph, i], RR.at[ph, i, 1], sp=right).start()
+        remote(src, piece(ph, me, i), SL.at[ph, i], RL.at[ph, i, 1], sp=left).start()
+
+    def to_pair(ph, origin, i):
+        if cuts[ph][i][3]:
+            k = rem(lax.div(origin, jnp.int32(SUB)) - gz + ng, ng)
+            part = piece(ph, origin, i)
+            remote(part, part, SY.at[ph, i], RY.at[ph, i, k], grp=pair).start()
+
+    def from_pair(ph, k):
+        rows = (SUB if k else SUB - 1) * UNIT
+        for i, (_, _, n_col, shared) in enumerate(cuts[ph]):
+            if shared:
+                drain(weights[ph].at[pl.ds(0, rows), pl.ds(0, n_col)], RY.at[ph, i, k])
+
+    def tick(h, fill=()):
+        fill = list(fill)
+        slots = 2 * len(order)
+
+        def work(n):
+            for f in fill[n * len(fill) // slots : (n + 1) * len(fill) // slots]:
+                f()
+
         from_left, from_right = rem(me - h + nz, nz), rem(me + h, nz)
-        for i in reversed(range(n_pieces)):
+        for n, (ph, i) in enumerate(order):
             a, b = piece(ph, from_left, i), piece(ph, from_right, i)
             remote(a, a, SR.at[ph, i], RR.at[ph, i, h], sp=right).wait_recv()
 
@@ -114,8 +138,8 @@
             def _():
                 remote(a, a, SR.at[ph, i], RR.at[ph, i, h + 1], sp=right).start()
 
-            if share and i == n_pieces - 1:
-                to_pair(ph, from_left)
+            to_pair(ph, from_left, i)
+            work(2 * n)
 
             @pl.when(h <= n_left)
             def _():
@@ -125,17 +149,19 @@
                 def _():
                     remote(b, b, SL.at[ph, i], RL.at[ph, i, h + 1], sp=left).start()
 
-                if share and i == n_pieces - 1:
-                    to_pair(ph, from_right)
-
-    def ticks(ph, first, last):
+                to_pair(ph, from_right, i)
+
+            work(2 * n + 1)
+
+    def ticks(first, last):
         def body(h, _):
-            tick(ph, h)
+            tick(h)
             return 0
 
         lax.fori_loop(first, last + 1, body, 0)
 
-    hop0(0)
+    for ph, i in order:
+        hop0(ph, i)
 
     waits = []
 
@@ -217,12 +243,6 @@
     WO[pl.ds(pl.multiple_of(t * dh, dh), dh), :] = wo_in[...]
     RES[pl.ds(pl.multiple_of(t * own_rows, own_rows), own_rows), :] = res_in[...]
 
-    first = n_right - 2 * (ng - 1)
-    ticks(0, 1, first)
-    for d in range(1, SUB):
-        slot = AR.at[rem(j - d + SUB, SUB)]
-        remote(slot, slot, SA.at[d], RA.at[d], sp=right).wait_recv()
-
     def member(i):
         return AR[i, 0:srows, :], AR[i, srows : srows + 1, :], AR[i, srows + 1 : srows + 2, :]
 
@@ -231,60 +251,84 @@
         new_top = jnp.maximum(part_total + top, part_top)
         return jnp.exp(part_total + top - new_top) * state + jnp.exp(part_top - new_top) * part, new_top
 
-    g_state, g_total, g_top = member(0)
-    for i in range(1, SUB):
-        m_state = member(i)
-        g_state, g_top = fold(g_state, g_top, m_state)
-        g_total = g_total + m_state[1]
-    GX[0:srows, :] = g_state
-    GX[srows : srows + 1, :] = g_total
-    GX[srows + 1 : srows + 2, :] = g_top
-
-    def chain(r):
-        @pl.when(gz == r)
+    def group_state():
+        for d in range(1, SUB):
+            slot = AR.at[rem(j - d + SUB, SUB)]
+            remote(slot, slot, SA.at[d], RA.at[d], sp=right).wait_recv()
+        g_state, g_total, g_top = member(0)
+        for i in range(1, SUB):
+            m_state = member(i)
+            g_state, g_top = fold(g_state, g_top, m_state)
+            g_total = g_total + m_state[1]
+        GX[0:srows, :] = g_state
+        GX[srows : srows + 1, :] = g_total
+        GX[srows + 1 : srows + 2, :] = g_top
+
+    def chain():
+        @pl.when(gz > 0)
         def _():
-            @pl.when(gz > 0)
-            def _():
-                remote(BR, BR, SB.at[0], RB.at[0], sp=right).wait_recv()
-
-            @pl.when(gz == 0)
-            def _():
-                BR[...] = jnp.zeros_like(BR)
-
-            state, top = BR[0:srows, :], BR[srows + 1 : srows + 2, :]
-            after, after_top = fold(
-                state, top, (GX[0:srows, :], GX[srows : srows + 1, :], GX[srows + 1 : srows + 2, :])
-            )
-            BS[0:srows, :] = after
-            BS[srows + 1 : srows + 2, :] = after_top
-
-            @pl.when(gz < ng - 1)
-            def _():
-                remote(BS, BR, SB.at[0], RB.at[0], sp=rem(me + SUB, nz)).start()
-
-            for i in range(SUB):
-                CS[i, 0:srows, :] = state
-                CS[i, srows + 1 : srows + 2, :] = top
-                if i < SUB - 1:
-                    state, top = fold(state, top, member(i))
-            for d in range(1, SUB):
-                i = rem(j + d, SUB)
-                remote(CS.at[i], CR.at[j], SC.at[d], RC.at[d], sp=gz * SUB + i).start()
-            CR[j] = CS[j]
-
-    def chain_step(r, _):
-        chain(r)
-        tick(0, first + 1 + 2 * r)
-        tick(0, first + 2 + 2 * r)
+            remote(BR, BR, SB.at[0], RB.at[0], sp=right).wait_recv()
+
+        @pl.when(gz == 0)
+        def _():
+            BR[...] = jnp.zeros_like(BR)
+
+        state, top = BR[0:srows, :], BR[srows + 1 : srows + 2, :]
+        after, after_top = fold(
+            state, top, (GX[0:srows, :], GX[srows : srows + 1, :], GX[srows + 1 : srows + 2, :])
+        )
+        BS[0:srows, :] = after
+        BS[srows + 1 : srows + 2, :] = after_top
+
+        @pl.when(gz < ng - 1)
+        def _():
+            remote(BS, BR, SB.at[0], RB.at[0], sp=rem(me + SUB, nz)).start()
+
+        for i in range(SUB):
+            CS[i, 0:srows, :] = state
+            CS[i, srows + 1 : srows + 2, :] = top
+            if i < SUB - 1:
+                state, top = fold(state, top, member(i))
+        for d in range(1, SUB):
+            i = rem(j + d, SUB)
+            remote(CS.at[i], CR.at[j], SC.at[d], RC.at[d], sp=gz * SUB + i).start()
+        CR[j] = CS[j]
+
+    early, first = ng - CHAIN_LATE, 2
+
+    @pl.when(gz < early)
+    def _():
+        group_state()
+        chain()
+
+    ticks(1, first)
+
+    @pl.when(gz >= early)
+    def _():
+        group_state()
+
+    def chain_tick(r, _):
+        tick(first + 1 + r)
+
+        @pl.when(gz == early + r)
+        def _():
+            chain()
+
         return 0
 
-    lax.fori_loop(0, ng - 2, chain_step, 0)
-    hop0(1)
-    chain_step(ng - 2, 0)
-    chain(ng - 1)
-    pass_on(0, res_rows)
-    pass_on(1, wo_rows)
-    tick(1, 1)
+    lax.fori_loop(0, CHAIN_LATE, chain_tick, 0)
+    at_tick = first + CHAIN_LATE
+
+    def next_tick(fill=()):
+        nonlocal at_tick
+        if at_tick < n_right:
+            at_tick += 1
+            tick(at_tick, fill)
+        else:
+            for f in fill:
+                f()
+
+    next_tick()
 
     for d in range(1, SUB):
         slot = CR.at[rem(j - d + SUB, SUB)]
@@ -295,7 +339,7 @@
         jnp.int32, (BLOCK, BLOCK), 1
     )
     mine = pl.ds(pl.multiple_of(t * dh, dh), dh)
-    for b in range(nb):
+    def hidden_block(b):
         cols = slice(b * BLOCK, (b + 1) * BLOCK)
         cum = ST[b : b + 1, :]
         if b == 0:
@@ -316,58 +360,66 @@
         gate = jax.nn.sigmoid(og_ref[cols, :].astype(F32))
         mixed = hidden * lax.rsqrt(mean_sq + NORM_EPS) * hng_ref[...] * gate
         MIX[cols, mine] = mixed.astype(BF16)
+
+    next_tick([functools.partial(hidden_block, b) for b in range(nb)])
     spread(2, mix_cols(t), mix_cols)
-    ticks(1, 2, 4)
+    next_tick()
+    pass_on(0, res_rows)
+    pass_on(1, wo_rows)
     pass_on(2, mix_cols)
-    for which, region in ((0, res_rows), (1, wo_rows)):
-        passed(which, region)
-    tick(1, 5)
-    passed(2, mix_cols)
+    next_tick()
+    for which, rows in ((0, res_rows), (1, wo_rows), (2, mix_cols)):
+        passed(which, rows)
 
     SSQ[...] = jnp.zeros_like(SSQ)
 
-    def project(n, _):
-        at = pl.ds(pl.multiple_of(n * 256, 256), 256)
+    def project(n):
+        at = slice(n * 256, (n + 1) * 256)
         branch = jnp.dot(MIX[...], WO[:, at], preferred_element_type=F32)
         mid = (RES[:, at].astype(F32) + branch).astype(BF16)
         MID[:, at] = mid
         wide = mid.astype(F32)
         SSQ[...] += wide[:, :128] * wide[:, :128] + wide[:, 128:] * wide[:, 128:]
-        return 0
-
-    n_cols = width // 256
-    for n in range(0, n_cols, 4):
-        lax.fori_loop(n, n + 4, project, 0)
-        tick(1, 6 + n // 4)
-
-    def normalize(n, _):
-        at = pl.ds(pl.multiple_of(n * 64, 64), 64)
+
+    def normalize(n):
+        at = slice(n * 64, (n + 1) * 64)
         mean_sq = jnp.sum(SSQ[at, :], axis=1, keepdims=True) / width
         NRM[at, :] = (MID[at, :].astype(F32) * lax.rsqrt(mean_sq + NORM_EPS) * fng_ref[...]).astype(BF16)
-        return 0
-
-    lax.fori_loop(0, tok // 64, normalize, 0)
-    tick(1, 8)
-
-    if share:
-        drain(UP.at[pl.ds(0, (nz - 1) * UNIT), :], RYU.at[0])
-
-    def upward(n, _):
-        at = pl.ds(pl.multiple_of(n * 256, 256), 256)
-        value = jnp.maximum(jnp.dot(NRM[...], UP[:, at], preferred_element_type=F32), 0.0)
-        ACT[:, at] = (value * value).astype(BF16)
-        return 0
-
-    for n in range(0, hid // 256, 2):
-        lax.fori_loop(n, n + 2, upward, 0)
-        tick(1, 9 + n // 2)
+
+    n_cols = width // 256
+    projects = [functools.partial(project, n) for n in range(n_cols)]
+    next_tick(projects[: n_cols // 2])
+    next_tick(projects[n_cols // 2 :])
+    next_tick([functools.partial(normalize, n) for n in range(tok // 64)])
 
     def group_of(k):
         return rem(gz + k, ng)
 
+    def upward(k, n, final):
+        at = slice(n * hid_half, (n + 1) * hid_half)
+        rows = pl.ds(pl.multiple_of(group_of(k) * gcols, gcols), gcols)
+        value = jnp.dot(NRM[:, rows], UP[rows, at], preferred_element_type=F32)
+        if k:
+            value = value + UACC[:, at]
+        if final:
+            value = jnp.maximum(value, 0.0)
+            ACT[:, at] = (value * value).astype(BF16)
+        else:
+            UACC[:, at] = value
+
+    def ups(k, final=False):
+        first_half = functools.partial(upward, k, 0, final)
+
+        def start():
+            if share:
+                from_pair(0, k)
+            first_half()
+
+        return [start, functools.partial(upward, k, 1, final)]
+
     def down(k):
         if share:
-            drain(DN.at[pl.ds(0, (SUB if k else SUB - 1) * UNIT), :], RYD.at[k])
+            from_pair(1, k)
         rows = pl.ds(pl.multiple_of(group_of(k) * gcols, gcols), gcols)
         value = lax.dot_general(
             ACT[...], DN[rows, :], (((1,), (1,)), ((), ())), preferred_element_type=F32
@@ -398,36 +450,41 @@
             value = value + RSR[k, rem(x - d + nx, nx)].astype(F32)
         out_ref[:, at] = value.astype(BF16)
 
-    done, order = 8 + hid // 512, []
-    plan = [(0, 3)]
-    for s in range(1, ng // 2):
-        plan += [(ng - s, SUB * s + 3), (s, SUB * s + 3)]
-    plan += [(ng // 2, n_right)]
-    late = 0
-    for n, (k, need) in enumerate(plan):
-        while done < need:
-            done += 1
-            tick(1, done)
+    turn = [0]
+    for n in range(1, ng // 2):
+        turn += [ng - n, n]
+    turn += [ng // 2]
+    ready = [SUB - 1] + [SUB * (n // 2 + 1) + SUB - 1 for n in range(ng - 2)] + [n_right]
+    left_up = list(turn)
+    while at_tick < n_right:
+        n_ready = sum(ready[turn.index(k)] <= at_tick for k in left_up[:-1])
+        per = min(n_ready, -(-len(left_up[:-1]) // (n_right - at_tick)))
+        fill = []
+        for k in left_up[:per]:
+            fill += ups(k)
+        left_up = left_up[per:]
+        next_tick(fill)
+    for k in left_up:
+        for f in ups(k, final=k == turn[-1]):
+            f()
+    for n, k in enumerate(turn):
         down(k)
-        if done < n_right and n < len(plan) - 1 and done < 14:
-            done += 1
-            tick(1, done)
-        order.append(k)
-        if n > 0:
-            add_up(order[n - 1])
-        if n > 3:
-            finish(order[late])
-            late += 1
-    add_up(order[-1])
-    for k in order[late:]:
+        if n > 1:
+            add_up(turn[n - 2])
+        if n > 4:
+            finish(turn[n - 5])
+    for k in turn[-2:]:
+        add_up(k)
+    for k in turn[ng - 5 :]:
         finish(k)
 
-    for ph in range(2):
-        for i in range(n_pieces):
-            drain(weights[ph].at[pl.ds(0, n_right * UNIT), :], SR.at[ph, i])
-            drain(weights[ph].at[pl.ds(0, n_left * UNIT), :], SL.at[ph, i])
-        if share:
-            drain(weights[ph].at[pl.ds(0, (nz - 1) * UNIT), :], SY.at[ph])
+    for ph, i in order:
+        n_col, shared = cuts[ph][i][2:]
+        cols = pl.ds(0, n_col)
+        drain(weights[ph].at[pl.ds(0, n_right * UNIT), cols], SR.at[ph, i])
+        drain(weights[ph].at[pl.ds(0, n_left * UNIT), cols], SL.at[ph, i])
+        if shared:
+            drain(weights[ph].at[pl.ds(0, (nz - 1) * UNIT), cols], SY.at[ph, i])
     for copy in waits:
         copy.wait_send()
     for d in range(1, SUB):
@@ -474,6 +531,7 @@
         vmem((tok, width), BF16),
         vmem((tok, width), BF16),
         vmem((tok, 128), F32),
+        vmem((tok, hid), F32),
         vmem((tok, hid), BF16),
         vmem((ng, nx, CORES, own_rows, gcols), BF16),
         vmem((ng, nx, own_rows, gcols), BF16),
@@ -492,9 +550,8 @@
         dma((2, n_pieces, n_right + 1)),
         dma((2, n_pieces)),
         dma((2, n_pieces, n_right + 1)),
-        dma((2,)),
-        dma((1,)),
-        dma((ng,)),
+        dma((2, n_pieces)),
+        dma((2, n_pieces, ng)),
         dma((3, nx)),
         dma((3, nx)),
         dma((3, nx)),

time: 174 us -> 149 us (0.86)
  Pallas kernels: 172 us -> 147 us
    pallas_call x1, Pallas kernels: 172 us -> 147 us  [shards(): pl.pallas_call(functools.partial(kernel, sizes), out_shape=jax.ShapeDtype...]
where the time goes in v2:
time: 149 us
  Pallas kernels  147 us (99%)
  local copies, waits for them, and re-layouts  1.67 us (1%)
    pallas_call x1, Pallas kernels, shards(): pl.pallas_call(functools.partial(kernel, sizes), out_shape=jax.ShapeDtype...  147 us

profile of v2, /device:TPU:33, one launch (start us, length us, event | category | flops | bytes accessed | tf_op | source)
XLA Modules:
  0.0 149.0 jit_solution(5793249893289140020)
XLA Ops:
  0.0 147.4 %layer.1 = bf16[64,2048]{1,0:T(8,128)(2,1)} custom-call(bf16[512,128]{1,0:T(8,128)(2,1)} %q_ref.1, bf16[512,128]{1,0:T(8,128)(2,1)} %k_ref.1, bf16[512,128]{1,0:T(8,128)(2,1)} %v_ref.1, bf16[512,128]{1,0:T(8,128)(2,1)} %og_ref.1, f32[1,512]{1,0:T(1,128)} %ig_ref.1, f32[1,512]{1,0:T(1,128)} %fg_ref.1, f32[1,512]{1,0:T(1,128)} %ex_ref.1, f32[1,128]{1,0:T(1,128)} %bitcast.5, ...), custom_call_target="tpu_custom_call" | custom-call | tf_op jit(solution)/shard_map/layer/pallas_call | solution.py:570
  147.4 1.7 %copy.15 = bf16[64,2048]{1,0:T(8,128)(2,1)} copy(bf16[64,2048]{1,0:T(8,128)(2,1)} %layer.1) | data formatting | bytes 524288

commit v3 on v2

--- a/solution.py
+++ b/solution.py
@@ -8,7 +8,7 @@
 from jax.sharding import PartitionSpec as P
 
 BLOCK = 128
-CHAIN_LATE = 7
+CHAIN_LATE = 5
 CORES = 2
 SUB = 4
 UNIT = 16
@@ -40,8 +40,8 @@
     sizes,
     q_ref, k_ref, v_ref, og_ref, ig_ref, fg_ref, ex_ref, hng_ref, wo_in, res_in, fng_ref, up_in, dn_in,
     out_ref,
-    UP, DN, WO, RES, MIX, MID, NRM, SSQ, UACC, ACT, PART, SIB, SUM, RSR, LM, ST, AS, AR, GX, BS, BR, CS, CR,
-    SR, RR, SL, RL, SY, RY, SX, RX, SD, RD, SA, RA, SB, RB, SC, RC, SP, RP, SQ, RQ,
+    UP, DN, WO, RES, OWN, MIX, MID, NRM, SSQ, UACC, ACT, PART, SIB, SUM, RSR, LM, ST, AS, AR, GX, BS, BR, CS, CR,
+    SR, RR, SL, RL, SY, RY, SX, RX, SD, RD, SN, RN, SA, RA, SB, RB, SC, RC, SP, RP, SQ, RQ, WRAP,
 ):
     nz, nt, share = sizes
     nx = nt // CORES
@@ -71,134 +71,30 @@
         pltpu.make_async_copy(ref, ref, sem).wait()
 
     barrier = pltpu.get_barrier_semaphore()
-    others = [dict(sp=right), dict(sp=left), dict(sp=rem(me + SUB, nz)), dict(sp=rem(me + nz - SUB, nz))]
-    others += [dict(sp=gz * SUB + rem(j + d, SUB)) for d in range(1, SUB)]
-    others += [dict(tp=rem(x + d, nx) * CORES + c) for d in range(1, nx)]
-    others += [dict(tp=sib)]
+
+    def greet(**device):
+        pl.semaphore_signal(barrier, inc=1, device_id=device, device_id_type=MESH)
+
+    around_here = [dict(sp=gz * SUB + rem(j + d, SUB)) for d in range(1, SUB)]
+    around_here += [dict(tp=rem(x + d, nx) * CORES + c) for d in range(1, nx)]
+    around_here += [dict(tp=rem(x + d, nx) * CORES + 1 - c) for d in range(nx)]
     if share:
-        others += [dict(grp=pair)]
-    for device in others:
-        pl.semaphore_signal(barrier, inc=1, device_id=device, device_id_type=MESH)
-    pl.semaphore_wait(barrier, len(others))
-
-    hid_half = hid // 2
-    if share:
-        mine_row, mine_col = parity * UNIT, parity * hid_half
-        cuts = (
-            [(3 * UNIT, 0, hid, False), (2 * UNIT, mine_col, hid_half, True), (mine_row, 0, hid, True)],
-            [(2 * UNIT, 0, hid, False), (3 * UNIT, 0, hid, False), (mine_row, 0, hid, True)],
-        )
-        order = [(0, 2), (1, 2), (0, 1), (1, 1), (0, 0), (1, 0)]
-    else:
-        cuts = ([(i * UNIT, 0, hid, False) for i in range(4)],) * 2
-        order = [(ph, i) for i in range(4) for ph in range(2)]
-    weights, own_w = (UP, DN), (up_in, dn_in)
-
-    def region(ref, start, ph, i):
-        row, col, n_col, _ = cuts[ph][i]
-        row = pl.multiple_of(start + row, UNIT)
-        if n_col == hid:
-            return ref.at[pl.ds(row, UNIT), :]
-        return ref.at[pl.ds(row, UNIT), pl.ds(pl.multiple_of(col, 128), n_col)]
-
-    def piece(ph, origin, i):
-        return region(weights[ph], origin * wrows, ph, i)
-
-    def hop0(ph, i):
-        src = region(own_w[ph], 0 * me, ph, i)
-        remote(src, piece(ph, me, i), SR.at[ph, i], RR.at[ph, i, 1], sp=right).start()
-        remote(src, piece(ph, me, i), SL.at[ph, i], RL.at[ph, i, 1], sp=left).start()
-
-    def to_pair(ph, origin, i):
-        if cuts[ph][i][3]:
-            k = rem(lax.div(origin, jnp.int32(SUB)) - gz + ng, ng)
-            part = piece(ph, origin, i)
-            remote(part, part, SY.at[ph, i], RY.at[ph, i, k], grp=pair).start()
-
-    def from_pair(ph, k):
-        rows = (SUB if k else SUB - 1) * UNIT
-        for i, (_, _, n_col, shared) in enumerate(cuts[ph]):
-            if shared:
-                drain(weights[ph].at[pl.ds(0, rows), pl.ds(0, n_col)], RY.at[ph, i, k])
-
-    def tick(h, fill=()):
-        fill = list(fill)
-        slots = 2 * len(order)
-
-        def work(n):
-            for f in fill[n * len(fill) // slots : (n + 1) * len(fill) // slots]:
-                f()
-
-        from_left, from_right = rem(me - h + nz, nz), rem(me + h, nz)
-        for n, (ph, i) in enumerate(order):
-            a, b = piece(ph, from_left, i), piece(ph, from_right, i)
-            remote(a, a, SR.at[ph, i], RR.at[ph, i, h], sp=right).wait_recv()
-
-            @pl.when(h < n_right)
-            def _():
-                remote(a, a, SR.at[ph, i], RR.at[ph, i, h + 1], sp=right).start()
-
-            to_pair(ph, from_left, i)
-            work(2 * n)
-
-            @pl.when(h <= n_left)
-            def _():
-                remote(b, b, SL.at[ph, i], RL.at[ph, i, h], sp=left).wait_recv()
-
-                @pl.when(h < n_left)
-                def _():
-                    remote(b, b, SL.at[ph, i], RL.at[ph, i, h + 1], sp=left).start()
-
-                to_pair(ph, from_right, i)
-
-            work(2 * n + 1)
-
-    def ticks(first, last):
-        def body(h, _):
-            tick(h)
-            return 0
-
-        lax.fori_loop(first, last + 1, body, 0)
-
-    for ph, i in order:
-        hop0(ph, i)
-
-    waits = []
-
-    def wo_rows(s):
-        return WO.at[pl.ds(pl.multiple_of(s * dh, dh), dh), :]
-
-    def res_rows(s):
-        return RES.at[pl.ds(pl.multiple_of(s * own_rows, own_rows), own_rows), :]
-
-    def mix_cols(s):
-        return MIX.at[:, pl.ds(pl.multiple_of(s * dh, dh), dh)]
-
-    def spread(which, own, region):
-        for d in [2, 1, 3, *range(4, nx)]:
-            if d < nx:
-                copy = remote(own, region(t), SX.at[which, d], RX.at[which, d], tp=rem(x + d, nx) * CORES + c)
-                copy.start()
-                waits.append(copy)
-        copy = remote(own, region(t), SD.at[which, 0], RD.at[which, 0], tp=sib)
-        copy.start()
-        waits.append(copy)
-
-    def pass_on(which, region):
-        for d in range(1, nx):
-            part = region(rem(x - d + nx, nx) * CORES + c)
-            remote(part, part, SX.at[which, d], RX.at[which, d], tp=sib).wait_recv()
-            copy = remote(part, part, SD.at[which, d], RD.at[which, d], tp=sib)
-            copy.start()
-            waits.append(copy)
-
-    def passed(which, region):
-        for d in range(nx):
-            part = region(rem(x - d + nx, nx) * CORES + 1 - c)
-            remote(part, part, SD.at[which, d], RD.at[which, d], tp=sib).wait_recv()
-
-    spread(0, res_in, res_rows)
-    spread(1, wo_in, wo_rows)
+        around_here += [dict(grp=pair)]
+    for device in around_here:
+        greet(**device)
+    greet(sp=left)
+
+    @pl.when(me < nz - 1)
+    def _():
+        greet(sp=right)
+
+    @pl.when(gz < ng - 1)
+    def _():
+        greet(sp=me + SUB)
+
+    @pl.when(gz > 0)
+    def _():
+        greet(sp=me - SUB)
 
     lane = lax.broadcasted_iota(jnp.int32, (1, BLOCK), 1)
     scale = dh ** (-0.5)
@@ -232,16 +128,159 @@
         AS[i, 0:srows, :] = memory[i * srows : (i + 1) * srows, :]
         AS[i, srows : srows + 1, :] = jnp.broadcast_to(total, (1, dh))
         AS[i, srows + 1 : srows + 2, :] = jnp.broadcast_to(top, (1, dh))
+    pl.semaphore_wait(
+        barrier, len(around_here) + 1 + lax.min(me, 1) + lax.min(ng - 1 - gz, 1) + lax.min(gz, 1)
+    )
+
+    @pl.when(me == nz - 1)
+    def _():
+        pl.semaphore_signal(WRAP, inc=1, device_id=dict(sp=right), device_id_type=MESH)
+
+    waits = []
     for d in range(1, SUB):
         i = rem(j + d, SUB)
         copy = remote(AS.at[i], AR.at[j], SA.at[d], RA.at[d], sp=gz * SUB + i)
         copy.start()
         waits.append(copy)
     AR[j] = AS[j]
+
+    hid_half = hid // 2
+    if share:
+        mine_row, mine_col = parity * UNIT, parity * hid_half
+        cuts = (
+            [(3 * UNIT, 0, hid, False), (2 * UNIT, mine_col, hid_half, True), (mine_row, 0, hid, True)],
+            [(2 * UNIT, 0, hid, False), (3 * UNIT, 0, hid, False), (mine_row, 0, hid, True)],
+        )
+        order = [(0, 2), (1, 2), (0, 1), (1, 1), (0, 0), (1, 0)]
+    else:
+        cuts = ([(i * UNIT, 0, hid, False) for i in range(4)],) * 2
+        order = [(ph, i) for i in range(4) for ph in range(2)]
+    weights, own_w = (UP, DN), (up_in, dn_in)
+
+    def region(ref, start, ph, i):
+        row, col, n_col, _ = cuts[ph][i]
+        row = pl.multiple_of(start + row, UNIT)
+        if n_col == hid:
+            return ref.at[pl.ds(row, UNIT), :]
+        return ref.at[pl.ds(row, UNIT), pl.ds(pl.multiple_of(col, 128), n_col)]
+
+    def piece(ph, origin, i):
+        return region(weights[ph], origin * wrows, ph, i)
+
+    def hop0(to_right):
+        for ph, i in order:
+            src = region(own_w[ph], 0 * me, ph, i)
+            if to_right:
+                remote(src, piece(ph, me, i), SR.at[ph, i], RR.at[ph, i, 1], sp=right).start()
+            else:
+                remote(src, piece(ph, me, i), SL.at[ph, i], RL.at[ph, i, 1], sp=left).start()
+
+    def to_pair(ph, origin, i):
+        if cuts[ph][i][3]:
+            k = rem(lax.div(origin, jnp.int32(SUB)) - gz + ng, ng)
+            part = piece(ph, origin, i)
+            remote(part, part, SY.at[ph, i], RY.at[ph, i, k], grp=pair).start()
+
+    def from_pair(ph, k):
+        rows = (SUB if k else SUB - 1) * UNIT
+        for i, (_, _, n_col, shared) in enumerate(cuts[ph]):
+            if shared:
+                drain(weights[ph].at[pl.ds(0, rows), pl.ds(0, n_col)], RY.at[ph, i, k])
+
+    def tick(h, fill=()):
+        fill = list(fill)
+        slots = 2 * len(order)
+
+        def work(n):
+            for f in fill[n * len(fill) // slots : (n + 1) * len(fill) // slots]:
+                f()
+
+        from_left, from_right = rem(me - h + nz, nz), rem(me + h, nz)
+        for n, (ph, i) in enumerate(order):
+            a, b = piece(ph, from_left, i), piece(ph, from_right, i)
+            remote(a, a, SR.at[ph, i], RR.at[ph, i, h], sp=right).wait_recv()
+
+            @pl.when(h < n_right)
+            def _():
+                remote(a, a, SR.at[ph, i], RR.at[ph, i, h + 1], sp=right).start()
+
+            to_pair(ph, from_left, i)
+            work(2 * n)
+
+            @pl.when(h <= n_left)
+            def _():
+                remote(b, b, SL.at[ph, i], RL.at[ph, i, h], sp=left).wait_recv()
+
+                @pl.when(h < n_left)
+                def _():
+                    remote(b, b, SL.at[ph, i], RL.at[ph, i, h + 1], sp=left).start()
+
+                to_pair(ph, from_right, i)
+
+            work(2 * n + 1)
+
+    def ticks(first, last):
+        def body(h, _):
+            tick(h)
+            return 0
+
+        lax.fori_loop(first, last + 1, body, 0)
+
+    hop0(True)
+
+    @pl.when(me > 0)
+    def _():
+        hop0(False)
+
+
+    def wo_rows(s):
+        return WO.at[pl.ds(pl.multiple_of(s * dh, dh), dh), :]
+
+    def res_rows(s):
+        return RES.at[pl.ds(pl.multiple_of(s * own_rows, own_rows), own_rows), :]
+
+    def mix_cols(s):
+        return pl.ds(pl.multiple_of(s * dh, dh), dh)
+
+    def around(d):
+        return rem(x + d, nx), rem(x - d + nx, nx)
+
+    hops = [d for d in [2, 1, 3, *range(4, nx)] if d < nx]
+
+    def begin(*args, **device):
+        copy = remote(*args, **device)
+        copy.start()
+        waits.append(copy)
+
+    for d in hops:
+        begin(res_in, res_rows(x), SX.at[0, d], RX.at[0, d], tp=around(d)[0] * CORES + c)
+    for d in hops:
+        begin(wo_in, wo_rows(t), SX.at[1, d], RX.at[1, d], tp=around(d)[0] * CORES + c)
+    begin(wo_in, wo_rows(t), SD.at[1, 0], RD.at[1, 0], tp=sib)
+
+    def pass_on():
+        for d in hops:
+            part = wo_rows(around(d)[1] * CORES + c)
+            remote(part, part, SX.at[1, d], RX.at[1, d], tp=sib).wait_recv()
+            begin(part, part, SD.at[1, d], RD.at[1, d], tp=sib)
+
+    def project_ready():
+        for d in hops:
+            part = res_rows(around(d)[1])
+            remote(part, part, SX.at[0, d], RX.at[0, d], tp=sib).wait_recv()
+        for d in range(nx):
+            part = wo_rows(around(d)[1] * CORES + 1 - c)
+            remote(part, part, SD.at[1, d], RD.at[1, d], tp=sib).wait_recv()
+        for d in range(nx):
+            here = around(d)[1] * CORES
+            if d:
+                drain(MIX.at[:, mix_cols(here + c)], RX.at[2, d])
+            drain(MIX.at[:, mix_cols(here + 1 - c)], RD.at[2, d])
+
     UP[pl.ds(pl.multiple_of(me * wrows, wrows), wrows), :] = up_in[...]
     DN[pl.ds(pl.multiple_of(me * wrows, wrows), wrows), :] = dn_in[...]
     WO[pl.ds(pl.multiple_of(t * dh, dh), dh), :] = wo_in[...]
-    RES[pl.ds(pl.multiple_of(t * own_rows, own_rows), own_rows), :] = res_in[...]
+    RES[pl.ds(pl.multiple_of(x * own_rows, own_rows), own_rows), :] = res_in[...]
 
     def member(i):
         return AR[i, 0:srows, :], AR[i, srows : srows + 1, :], AR[i, srows + 1 : srows + 2, :]
@@ -294,30 +333,19 @@
             remote(CS.at[i], CR.at[j], SC.at[d], RC.at[d], sp=gz * SUB + i).start()
         CR[j] = CS[j]
 
-    early, first = ng - CHAIN_LATE, 2
+    early = ng - CHAIN_LATE
 
     @pl.when(gz < early)
     def _():
         group_state()
         chain()
 
-    ticks(1, first)
-
-    @pl.when(gz >= early)
-    def _():
-        group_state()
-
-    def chain_tick(r, _):
-        tick(first + 1 + r)
-
-        @pl.when(gz == early + r)
-        def _():
-            chain()
-
-        return 0
-
-    lax.fori_loop(0, CHAIN_LATE, chain_tick, 0)
-    at_tick = first + CHAIN_LATE
+    @pl.when(me == 0)
+    def _():
+        pl.semaphore_wait(WRAP, 1)
+        hop0(False)
+
+    at_tick = 0
 
     def next_tick(fill=()):
         nonlocal at_tick
@@ -328,18 +356,39 @@
             for f in fill:
                 f()
 
+    def nothing():
+        pass
+
+    def chain_at(g):
+        @pl.when(gz == g)
+        def _():
+            chain()
+
     next_tick()
 
-    for d in range(1, SUB):
-        slot = CR.at[rem(j - d + SUB, SUB)]
-        remote(slot, slot, SC.at[d], RC.at[d], sp=right).wait_recv()
-    before = jnp.concatenate([CR[i, 0:srows, :] for i in range(SUB)], axis=0)
-    before_top = CR[0, srows + 1 : srows + 2, :]
+    @pl.when(gz >= early)
+    def _():
+        group_state()
+
+    chain_at(early)
+    for g in range(early + 1, ng, 2):
+        next_tick()
+        next_tick([functools.partial(chain_at, g), nothing])
+        if g + 1 < ng:
+            next_tick()
+            chain_at(g + 1)
+
+    def state_before():
+        for d in range(1, SUB):
+            slot = CR.at[rem(j - d + SUB, SUB)]
+            remote(slot, slot, SC.at[d], RC.at[d], sp=right).wait_recv()
+
     causal = lax.broadcasted_iota(jnp.int32, (BLOCK, BLOCK), 0) >= lax.broadcasted_iota(
         jnp.int32, (BLOCK, BLOCK), 1
     )
-    mine = pl.ds(pl.multiple_of(t * dh, dh), dh)
     def hidden_block(b):
+        before = jnp.concatenate([CR[i, 0:srows, :] for i in range(SUB)], axis=0)
+        before_top = CR[0, srows + 1 : srows + 2, :]
         cols = slice(b * BLOCK, (b + 1) * BLOCK)
         cum = ST[b : b + 1, :]
         if b == 0:
@@ -359,17 +408,24 @@
         mean_sq = jnp.mean(hidden * hidden, axis=1, keepdims=True)
         gate = jax.nn.sigmoid(og_ref[cols, :].astype(F32))
         mixed = hidden * lax.rsqrt(mean_sq + NORM_EPS) * hng_ref[...] * gate
-        MIX[cols, mine] = mixed.astype(BF16)
-
-    next_tick([functools.partial(hidden_block, b) for b in range(nb)])
-    spread(2, mix_cols(t), mix_cols)
+        mixed = mixed.astype(BF16)
+        half = slice(b * own_rows, (b + 1) * own_rows)
+        for core in range(CORES):
+            OWN[core, half, :] = mixed[core * own_rows : (core + 1) * own_rows, :]
+        MIX[half, mix_cols(t)] = OWN[c, half, :]
+        for d in [*hops, 0]:
+            there = around(d)[0] * CORES
+            dst = MIX.at[half, mix_cols(t)]
+            if d:
+                remote(OWN.at[c, half], dst, SX.at[2, d], RX.at[2, d], tp=there + c).start()
+            remote(OWN.at[1 - c, half], dst, SD.at[2, d], RD.at[2, d], tp=there + 1 - c).start()
+
+    blocks = [functools.partial(hidden_block, b) for b in range(nb)]
     next_tick()
-    pass_on(0, res_rows)
-    pass_on(1, wo_rows)
-    pass_on(2, mix_cols)
-    next_tick()
-    for which, rows in ((0, res_rows), (1, wo_rows), (2, mix_cols)):
-        passed(which, rows)
+    next_tick([nothing, state_before, blocks[0]])
+    next_tick(blocks[1:])
+    next_tick([pass_on, nothing])
+    next_tick([nothing, project_ready])
 
     SSQ[...] = jnp.zeros_like(SSQ)
 
@@ -382,40 +438,54 @@
         SSQ[...] += wide[:, :128] * wide[:, :128] + wide[:, 128:] * wide[:, 128:]
 
     def normalize(n):
-        at = slice(n * 64, (n + 1) * 64)
+        at = slice(n * own_rows, (n + 1) * own_rows)
+        rows = pl.ds(pl.multiple_of((n * CORES + c) * own_rows, own_rows), own_rows)
         mean_sq = jnp.sum(SSQ[at, :], axis=1, keepdims=True) / width
-        NRM[at, :] = (MID[at, :].astype(F32) * lax.rsqrt(mean_sq + NORM_EPS) * fng_ref[...]).astype(BF16)
+        NRM[rows, :] = (MID[at, :].astype(F32) * lax.rsqrt(mean_sq + NORM_EPS) * fng_ref[...]).astype(BF16)
+        begin(NRM.at[rows, :], NRM.at[rows, :], SN.at[n], RN.at[n], tp=sib)
+
+    def normed_ready():
+        for n in range(nx):
+            rows = pl.ds(pl.multiple_of((n * CORES + 1 - c) * own_rows, own_rows), own_rows)
+            remote(NRM.at[rows, :], NRM.at[rows, :], SN.at[n], RN.at[n], tp=sib).wait_recv()
 
     n_cols = width // 256
-    projects = [functools.partial(project, n) for n in range(n_cols)]
-    next_tick(projects[: n_cols // 2])
-    next_tick(projects[n_cols // 2 :])
-    next_tick([functools.partial(normalize, n) for n in range(tok // 64)])
+    next_tick([functools.partial(project, n) for n in range(n_cols // 2)])
+    next_tick([functools.partial(project, n) for n in range(n_cols // 2, n_cols)])
+    next_tick([functools.partial(normalize, n) for n in range(nx)])
+    normed_ready()
 
     def group_of(k):
         return rem(gz + k, ng)
 
-    def upward(k, n, final):
-        at = slice(n * hid_half, (n + 1) * hid_half)
-        rows = pl.ds(pl.multiple_of(group_of(k) * gcols, gcols), gcols)
-        value = jnp.dot(NRM[:, rows], UP[rows, at], preferred_element_type=F32)
-        if k:
-            value = value + UACC[:, at]
+    turn = [0]
+    for n in range(1, ng // 2):
+        turn += [ng - n, n]
+    turn += [ng // 2]
+
+    def upward(ks, n, n_col, final):
+        at = slice(n * n_col, (n + 1) * n_col)
+        value = None
+        for k in ks:
+            rows = pl.ds(pl.multiple_of(group_of(k) * gcols, gcols), gcols)
+            part = jnp.dot(NRM[:, rows], UP[rows, at], preferred_element_type=F32)
+            value = part if value is None else value + part
         if final:
-            value = jnp.maximum(value, 0.0)
+            value = jnp.maximum(value + UACC[:, at], 0.0)
             ACT[:, at] = (value * value).astype(BF16)
         else:
             UACC[:, at] = value
 
-    def ups(k, final=False):
-        first_half = functools.partial(upward, k, 0, final)
-
-        def start():
-            if share:
-                from_pair(0, k)
-            first_half()
-
-        return [start, functools.partial(upward, k, 1, final)]
+    near = 2 * ((n_right - SUB) // SUB) - 1
+    if share:
+        for k in turn[:near]:
+            from_pair(0, k)
+    next_tick([functools.partial(upward, turn[:near], n, 128, False) for n in range(hid // 128)])
+    if share:
+        for k in turn[near:]:
+            from_pair(0, k)
+    for n in range(hid // 256):
+        upward(turn[near:], n, 256, True)
 
     def down(k):
         if share:
@@ -442,7 +512,7 @@
 
     def finish(k):
         at = pl.ds(pl.multiple_of(group_of(k) * gcols, gcols), gcols)
-        value = MID[pl.ds(pl.multiple_of(t * own_rows, own_rows), own_rows), at].astype(F32)
+        value = MID[pl.ds(pl.multiple_of(x * own_rows, own_rows), own_rows), at].astype(F32)
         value = value + SUM[k, x].astype(F32)
         for d in range(1, nx):
             slot = RSR.at[k, rem(x - d + nx, nx)]
@@ -450,23 +520,6 @@
             value = value + RSR[k, rem(x - d + nx, nx)].astype(F32)
         out_ref[:, at] = value.astype(BF16)
 
-    turn = [0]
-    for n in range(1, ng // 2):
-        turn += [ng - n, n]
-    turn += [ng // 2]
-    ready = [SUB - 1] + [SUB * (n // 2 + 1) + SUB - 1 for n in range(ng - 2)] + [n_right]
-    left_up = list(turn)
-    while at_tick < n_right:
-        n_ready = sum(ready[turn.index(k)] <= at_tick for k in left_up[:-1])
-        per = min(n_ready, -(-len(left_up[:-1]) // (n_right - at_tick)))
-        fill = []
-        for k in left_up[:per]:
-            fill += ups(k)
-        left_up = left_up[per:]
-        next_tick(fill)
-    for k in left_up:
-        for f in ups(k, final=k == turn[-1]):
-            f()
     for n, k in enumerate(turn):
         down(k)
         if n > 1:
@@ -489,6 +542,10 @@
         copy.wait_send()
     for d in range(1, SUB):
         drain(CS.at[0], SC.at[d])
+    for d in range(nx):
+        if d:
+            drain(OWN.at[0], SX.at[2, d])
+        drain(OWN.at[0], SD.at[2, d])
 
     @pl.when(gz < ng - 1)
     def _():
@@ -526,11 +583,12 @@
         vmem((nz * wrows, hid), BF16),
         vmem((nz * wrows, hid), BF16),
         vmem((nt * dh, width), BF16),
+        vmem((nx * own_rows, width), BF16),
+        vmem((CORES, nx * own_rows, dh), BF16),
+        vmem((nx * own_rows, nt * dh), BF16),
+        vmem((nx * own_rows, width), BF16),
         vmem((tok, width), BF16),
-        vmem((tok, nt * dh), BF16),
-        vmem((tok, width), BF16),
-        vmem((tok, width), BF16),
-        vmem((tok, 128), F32),
+        vmem((nx * own_rows, 128), F32),
         vmem((tok, hid), F32),
         vmem((tok, hid), BF16),
         vmem((ng, nx, CORES, own_rows, gcols), BF16),
@@ -556,6 +614,8 @@
         dma((3, nx)),
         dma((3, nx)),
         dma((3, nx)),
+        dma((nx,)),
+        dma((nx,)),
         dma((SUB,)),
         dma((SUB,)),
         dma((1,)),
@@ -566,6 +626,7 @@
         dma((ng,)),
         dma((ng, nx)),
         dma((ng, nx)),
+        pltpu.SemaphoreType.REGULAR,
     ]
     return pl.pallas_call(
         functools.partial(kernel, sizes),

time: 149 us -> 146 us (0.980)
  Pallas kernels: 147 us -> 144 us
    pallas_call x1, Pallas kernels: 147 us -> 144 us  [shards(): pl.pallas_call(functools.partial(kernel, sizes), out_shape=jax.ShapeDtype...]
where the time goes in v3:
time: 146 us; the launch traced here: 145 us
  Pallas kernels  144 us (99%)
  local copies, waits for them, and re-layouts  1.67 us (1%)
    pallas_call x1, Pallas kernels, shards(): pl.pallas_call(functools.partial(kernel, sizes), out_shape=jax.ShapeDtype...  144 us

profile of v3, /device:TPU:33, one launch (start us, length us, event | category | flops | bytes accessed | tf_op | source)
XLA Modules:
  0.0 145.5 jit_solution(14694128001005371698)
XLA Ops:
  0.0 143.8 %layer.1 = bf16[64,2048]{1,0:T(8,128)(2,1)} custom-call(bf16[512,128]{1,0:T(8,128)(2,1)} %q_ref.1, bf16[512,128]{1,0:T(8,128)(2,1)} %k_ref.1, bf16[512,128]{1,0:T(8,128)(2,1)} %v_ref.1, bf16[512,128]{1,0:T(8,128)(2,1)} %og_ref.1, f32[1,512]{1,0:T(1,128)} %ig_ref.1, f32[1,512]{1,0:T(1,128)} %fg_ref.1, f32[1,512]{1,0:T(1,128)} %ex_ref.1, f32[1,128]{1,0:T(1,128)} %bitcast.5, ...), custom_call_target="tpu_custom_call" | custom-call | tf_op jit(solution)/shard_map/layer/pallas_call | solution.py:631
  143.8 1.7 %copy.15 = bf16[64,2048]{1,0:T(8,128)(2,1)} copy(bf16[64,2048]{1,0:T(8,128)(2,1)} %layer.1) | data formatting | bytes 524288

commit v4 on v3

--- a/solution.py
+++ b/solution.py
@@ -450,8 +450,7 @@
             remote(NRM.at[rows, :], NRM.at[rows, :], SN.at[n], RN.at[n], tp=sib).wait_recv()
 
     n_cols = width // 256
-    next_tick([functools.partial(project, n) for n in range(n_cols // 2)])
-    next_tick([functools.partial(project, n) for n in range(n_cols // 2, n_cols)])
+    next_tick([functools.partial(project, n) for n in range(n_cols)])
     next_tick([functools.partial(normalize, n) for n in range(nx)])
     normed_ready()
 
@@ -481,6 +480,8 @@
         for k in turn[:near]:
             from_pair(0, k)
     next_tick([functools.partial(upward, turn[:near], n, 128, False) for n in range(hid // 128)])
+    while at_tick < n_right:
+        next_tick()
     if share:
         for k in turn[near:]:
             from_pair(0, k)

time: 146 us -> 144 us (0.986)
  Pallas kernels: 144 us -> 142 us
    pallas_call x1, Pallas kernels: 144 us -> 142 us  [shards(): pl.pallas_call(functools.partial(kernel, sizes), out_shape=jax.ShapeDtype...]
where the time goes in v4:
time: 144 us
  Pallas kernels  142 us (99%)
  local copies, waits for them, and re-layouts  1.67 us (1%)
    pallas_call x1, Pallas kernels, shards(): pl.pallas_call(functools.partial(kernel, sizes), out_shape=jax.ShapeDtype...  142 us

profile of v4, /device:TPU:33, one launch (start us, length us, event | category | flops | bytes accessed | tf_op | source)
XLA Modules:
  0.0 143.9 jit_solution(4738204590464862607)
XLA Ops:
  0.0 142.2 %layer.1 = bf16[64,2048]{1,0:T(8,128)(2,1)} custom-call(bf16[512,128]{1,0:T(8,128)(2,1)} %q_ref.1, bf16[512,128]{1,0:T(8,128)(2,1)} %k_ref.1, bf16[512,128]{1,0:T(8,128)(2,1)} %v_ref.1, bf16[512,128]{1,0:T(8,128)(2,1)} %og_ref.1, f32[1,512]{1,0:T(1,128)} %ig_ref.1, f32[1,512]{1,0:T(1,128)} %fg_ref.1, f32[1,512]{1,0:T(1,128)} %ex_ref.1, f32[1,128]{1,0:T(1,128)} %bitcast.5, ...), custom_call_target="tpu_custom_call" | custom-call | tf_op jit(solution)/shard_map/layer/pallas_call | solution.py:632
  142.2 1.7 %copy.15 = bf16[64,2048]{1,0:T(8,128)(2,1)} copy(bf16[64,2048]{1,0:T(8,128)(2,1)} %layer.1) | data formatting | bytes 524288
